TPU v7x, 512 devices: a whole 4x8x8 slice. The times are simulated.
512 devices in a mesh: rep: 2 (over z_hi), fs: 32 (over z_lo, y), tp: 8 (over x, core).
Axes of the slice: x: 4, y: 8, z: 8 (z_hi: 2, z_lo: 4; z = z_hi * 4 + z_lo), core: 2. Of those that a mesh axis runs over, the one named last changes fastest.
Arguments:
- states: bfloat16 [24576, 2048], P(('rep', 'fs'), 'tp'), may hold values from -6 to 6
- mix_gain: float32 [2048], replicated, may hold values from 0.1 to 1.9
- w_value: bfloat16 [2048, 2048], P('fs', 'tp'), may hold values from -1 to 1
- w_gate: bfloat16 [2048, 2048], P('fs', 'tp'), may hold values from -0.125 to 0.125
- conv_kernel: float32 [31, 2048], replicated, may hold values from -1 to 1
- chan_gain: float32 [2048], replicated, may hold values from 0.1 to 1.9
- w_mix_out: bfloat16 [2048, 2048], P('fs', 'tp'), may hold values from -0.125 to 0.125
- mlp_gain: float32 [2048], replicated, may hold values from 0.1 to 1.9
- w_up: bfloat16 [2048, 6144], P('fs', 'tp'), may hold values from -0.125 to 0.125
- w_down_t: bfloat16 [2048, 6144], P('fs', 'tp'), may hold values from -0.078125 to 0.078125
Outputs:
- layer_out: bfloat16 [24576, 2048], P(('rep', 'fs'), 'tp')
All inputs are finite; a program needn't handle non-finite values.
Results may differ from a plain program's by a relative error of at most 0.017.
Values may be sent and summed in bfloat16 or wider, within the bound.
No kernel may reach another device: no remote copies, remote signals or barrier semaphores. Data moves between devices by JAX's collectives and lax.ppermute only.
A program may use at most 64 MiB of HBM per device.

v0:
```python
import jax
import jax.numpy as jnp
from jax import lax
from jax.sharding import Mesh
from jax.sharding import PartitionSpec as P

D = 2048
KWIDTH = 31
LENGTH = 128
TP = ("tp_0", "tp_1")
EPS = 1e-06


def cut_rows(length, count):
    hop = length // count
    if hop >= 8:
        hop -= hop % 8
    return [hop * k for k in range(1, count)]


def gather_in_order(shard, axes, order):
    pieces = shard
    for k in order:
        pieces = lax.all_gather(pieces, axes[k])
    done = order[::-1]
    back = [done.index(k) for k in range(len(axes))]
    pieces = pieces.transpose(*back, *range(len(axes), pieces.ndim))
    return pieces.reshape(-1, *shard.shape)


def laid_out(pieces, dim):
    pieces = jnp.moveaxis(pieces, 0, dim)
    dims = pieces.shape
    return pieces.reshape(*dims[:dim], dims[dim] * dims[dim + 1], *dims[dim + 2 :])


def gather_at_once(shard, axes, dim):
    split_at = max(range(max(1, shard.ndim - 1)), key=lambda d: shard.shape[d])
    count, outs = (len(axes), [])
    for initial, slab in enumerate(
        jnp.split(shard, cut_rows(shard.shape[split_at], count), axis=split_at)
    ):
        if slab.size:
            order = [(initial - k) % count for k in range(count)]
            outs.append(gather_in_order(slab, axes, order))
    return laid_out(jnp.concatenate(outs, axis=split_at + 1), dim)


def half_of(weight):
    width = weight.shape[1] // 2
    return lax.dynamic_slice_in_dim(weight, lax.axis_index("rep") * width, width, 1)


def whole_halves(weights):
    mine = jnp.concatenate([half_of(w) for w in weights], axis=1)
    pieces = lax.all_gather(mine, ("rep", "fs"), axis=0, tiled=True)
    pieces = pieces.reshape(2, -1, mine.shape[1])
    ends, at = ([], 0)
    for w in weights[:-1]:
        at += w.shape[1] // 2
        ends.append(at)
    return [jnp.split(pieces[r], ends, axis=1) for r in range(2)]


def copy_for_each(shard, axis):
    copies = jnp.broadcast_to(shard, (lax.axis_size(axis), *shard.shape))
    return lax.all_to_all(copies, axis, split_axis=0, concat_axis=0, tiled=True)


def over_copies(shard, axis):
    everything = copy_for_each(shard, axis)
    return jnp.sum(everything, axis=0)


def in_one(arrays, axis):
    ends = [0]
    for a in arrays:
        ends.append(ends[-1] + a.size)
    so_far = over_copies(jnp.concatenate([a.ravel() for a in arrays]), axis)
    return tuple((so_far[b:e].reshape(a.shape) for a, b, e in zip(arrays, ends, ends[1:])))


def in_blocks(shard, dim, count):
    before, after = (shard.shape[:dim], shard.shape[dim + 1 :])
    return jnp.moveaxis(shard.reshape(*before, count, -1, *after), dim, 0)


def summed_on_arrival(shard, axis, dim):
    count = lax.axis_size(axis)
    pieces = lax.all_to_all(in_blocks(shard, dim, count), axis, 0, 0, tiled=True)
    return jnp.sum(pieces.astype(jnp.float32), axis=0)


def collect(shard, axis, dim):
    pieces = copy_for_each(shard, axis)
    return laid_out(pieces, dim)


def rms_norm(rows, gain):
    values = rows.astype(jnp.float32)
    scaled = values * lax.rsqrt(jnp.mean(values * values, axis=-1, keepdims=True) + EPS)
    return (scaled * gain).astype(jnp.bfloat16)


def times_transposed(left, right):
    return lax.dot_general(
        left, right, (((1,), (1,)), ((), ())), preferred_element_type=jnp.float32
    )


def body(
    states, mix_gain, w_value, w_gate, conv_kernel, chan_gain, w_mix_out, mlp_gain, w_up, w_down_t
):
    width = states.shape[1]
    offset = lax.axis_index(TP) * width
    token_rows = states.shape[0]
    whole_rows = gather_at_once(states, TP, 1)
    normed = rms_norm(whole_rows, mix_gain)
    mix = whole_halves((w_value, w_gate, w_mix_out))
    value = jnp.concatenate(
        [jnp.dot(normed, h[0], preferred_element_type=jnp.float32) for h in mix], axis=1
    )
    gate = jnp.concatenate(
        [jnp.dot(normed, h[1], preferred_element_type=jnp.float32) for h in mix], axis=1
    )
    gated = value * jax.nn.sigmoid(gate)
    own_kernel = lax.dynamic_slice_in_dim(conv_kernel, offset, width, 1)
    blocks = gated.reshape(token_rows // LENGTH, LENGTH, width)
    padded = jnp.pad(blocks, ((0, 0), (KWIDTH - 1, 0), (0, 0)))
    filtered = jnp.zeros_like(blocks)
    for tap in range(KWIDTH):
        filtered = filtered + own_kernel[tap][None, None, :] * padded[:, tap : tap + LENGTH, :]
    filtered = filtered.reshape(token_rows, width)
    sum_rows, square_rows = in_one(
        (jnp.sum(filtered, axis=-1), jnp.sum(filtered * filtered, axis=-1)), TP
    )
    mean_rows = (sum_rows / D)[:, None]
    variance = (square_rows / D)[:, None] - mean_rows * mean_rows
    own_gain = lax.dynamic_slice_in_dim(chan_gain, offset, width, 0)
    activated = jax.nn.silu((filtered - mean_rows) * lax.rsqrt(variance + EPS) * own_gain).astype(
        jnp.bfloat16
    )
    mixer_terms = times_transposed(activated, jnp.concatenate([h[2] for h in mix], axis=1))
    mixed = summed_on_arrival(mixer_terms.astype(jnp.bfloat16), TP, 1)
    middle = (states.astype(jnp.float32) + mixed).astype(jnp.bfloat16)
    middle_rows = collect(middle, TP, 1)
    normed_mid = rms_norm(middle_rows, mlp_gain)
    fed_terms = 0.0
    for up, down in whole_halves((w_up, w_down_t)):
        upward = jnp.dot(normed_mid, up, preferred_element_type=jnp.float32)
        hidden = jnp.square(jnp.maximum(upward, 0.0)).astype(jnp.bfloat16)
        fed_terms = fed_terms + times_transposed(hidden, down)
    fed = summed_on_arrival(fed_terms.astype(jnp.bfloat16), TP, 1)
    return (middle.astype(jnp.float32) + fed).astype(jnp.bfloat16)


def solution(mesh):
    split = Mesh(
        mesh.devices.reshape(mesh.shape["rep"], mesh.shape["fs"], 4, 2),
        ("rep", "fs", "tp_0", "tp_1"),
    )
    return jax.shard_map(
        body,
        mesh=split,
        in_specs=(
            P(("rep", "fs"), TP),
            P(),
            P("fs", TP),
            P("fs", TP),
            P(),
            P(),
            P("fs", TP),
            P(),
            P("fs", TP),
            P("fs", TP),
        ),
        out_specs=P(("rep", "fs"), TP),
        check_vma=False,
    )
```

profile of v0, /device:TPU:1, one launch (start us, length us, event | category | flops | bytes accessed | tf_op | source)
XLA Modules:
  0.0 234.6 jit_solution(18182806777791911851)
XLA Ops:
  11.2 10.8 %all-gather = bf16[768,256]{1,0:T(8,128)(2,1)S(1)} all-gather(bf16[192,256]{1,0:T(8,128)(2,1)S(1)} %get-tuple-element.41), channel_id=2, replica_groups=mesh['rep'=2,'fs'=32,'tp_0'=4,'tp_1'=2] {'tp_0'}, dimensions={0}, use_global_device_ids=true | all-gather | bytes 491520 | tf_op jit(solution)/shard_map/all_gather | solution.py:24
  22.0 10.5 %all-gather.1 = bf16[8,192,256]{2,1,0:T(8,128)(2,1)S(1)} all-gather(bf16[4,192,256]{2,1,0:T(8,128)(2,1)S(1)} %bitcast.103), channel_id=3, replica_groups=mesh['rep'=2,'fs'=32,'tp_0'=4,'tp_1'=2] {'tp_1'}, dimensions={0}, use_global_device_ids=true | all-gather | bytes 1179648 | tf_op jit(solution)/shard_map/all_gather | solution.py:24
  32.6 2.0 all-gather.2
  34.6 11.2 %all-gather.3 = bf16[8,192,256]{2,1,0:T(8,128)(2,1)S(1)} all-gather(bf16[2,192,256]{2,1,0:T(8,128)(2,1)S(1)} %bitcast.104), channel_id=5, replica_groups=mesh['rep'=2,'fs'=32,'tp_0'=4,'tp_1'=2] {'tp_0'}, dimensions={0}, use_global_device_ids=true | all-gather | bytes 983040 | tf_op jit(solution)/shard_map/all_gather | solution.py:24
  47.0 1.8 copy.53
  48.9 2.3 reshape.149
  51.9 1.8 fusion
  54.7 1.3 constant_dynamic-slice_fusion
  56.1 2.2 multiply_convert_fusion
  58.3 38.9 %all-gather.7.cloned.1.call-done = bf16[4096,384]{1,0:T(8,128)(2,1)} async-done(((bf16[64,384]{1,0:T(8,128)(2,1)}), bf16[4096,384]{1,0:T(8,128)(2,1)}) %all-gather.7.cloned.1.call-update) | async-done | bytes 3145744 | tf_op jit(solution)/shard_map/all_gather | solution.py:56
  97.2 1.6 fusion.35
  98.8 1.6 fusion.36
  100.4 1.6 fusion.38
  102.1 1.6 fusion.37
  103.8 4.5 %fusion.109 = (f32[3,128]{1,0:T(4,128)S(1)}, f32[3,128]{1,0:T(4,128)S(1)}, f32[3,128,256]{1,2,0:T(8,128)S(1)}) fusion(f32[3,128,256]{1,2,0:T(8,128)S(1)} %maximum_multiply_fusion, f32[256]{0:T(256)S(1)} %bitcast.119, f32[256]{0:T(256)S(1)} %bitcast.121, f32[256]{0:T(256)S(1)} %bitcast.122, f32[256]{0:T(256)S(1)} %bitcast.123, f32[256]{0:T(256)S(1)} %bitcast.124, ...), kind=kLoop, calls=%fused_computation.159 | loop fusion | flops 6290688 | bytes 821248 | tf_op jit(solution)/shard_map/reduce_sum | solution.py:135
  109.0 8.6 %all-to-all-start = ((f32[8,1,768]{2,1,0:T(1,128)}), f32[8,1,768]{2,1,0:T(1,128)S(1)}, u32[]{:S(2)}, u32[]{:S(2)}) async-start(f32[8,1,768]{2,1,0:T(1,128)} %broadcast_in_dim.4), calls=%async_computation | async-start | bytes 49152 | tf_op jit(solution)/shard_map/all_to_all | solution.py:67
  117.6 1.3 fusion.111
  119.0 3.3 %all-to-all-done = f32[8,1,768]{2,1,0:T(1,128)S(1)} async-done(((f32[8,1,768]{2,1,0:T(1,128)}), f32[8,1,768]{2,1,0:T(1,128)S(1)}, u32[]{:S(2)}, u32[]{:S(2)}) %all-to-all-start) | async-done | bytes 24608 | tf_op jit(solution)/shard_map/all_to_all | solution.py:67
  123.3 23.8 %all_to_all.21 = bf16[8,384,256]{2,1,0:T(8,128)(2,1)S(1)} all-to-all(bf16[8,384,256]{2,1,0:T(8,128)(2,1)S(1)} %bitcast.98), channel_id=1, replica_groups=mesh['rep'=2,'fs'=32,'tp_0'=4,'tp_1'=2] {'tp_0','tp_1'}, dimensions={0} | all-to-all | bytes 3145728 | tf_op jit(solution)/shard_map/all_to_all | solution.py:90
  147.7 24.1 %all_to_all.22 = bf16[8,384,256]{1,2,0:T(8,128)(2,1)S(1)} all-to-all(bf16[8,384,256]{1,2,0:T(8,128)(2,1)S(1)} %broadcast_in_dim.5), channel_id=1, replica_groups=mesh['rep'=2,'fs'=32,'tp_0'=4,'tp_1'=2] {'tp_0','tp_1'}, dimensions={0} | all-to-all | bytes 3145728 | tf_op jit(solution)/shard_map/all_to_all | solution.py:67
  172.6 17.4 %all-gather.9.cloned.1.call-done = bf16[4096,768]{1,0:T(8,128)(2,1)} async-done(((bf16[64,768]{1,0:T(8,128)(2,1)}), bf16[4096,768]{1,0:T(8,128)(2,1)}) %all-gather.9.cloned.1.call-update) | async-done | bytes 6291472 | tf_op jit(solution)/shard_map/all_gather | solution.py:56
  190.0 5.4 %fusion.6 = f32[384,2048]{1,0:T(8,128)} fusion(bf16[4096,768]{1,0:T(8,128)(2,1)} %all-gather.9.cloned.1.call-done, bf16[384,2048]{0,1:T(8,128)(2,1)S(1)} %fusion.2), kind=kOutput, calls=%fused_computation.47 | convolution fusion | flops 1208401920 | bytes 7864320 | tf_op jit(solution)/shard_map/dot_general | solution.py:106
  195.4 4.7 %add_convert_fusion = bf16[384,2048]{1,0:T(8,128)(2,1)S(1)} fusion(f32[384,2048]{1,0:T(8,128)} %fusion.6, bf16[4096,768]{1,0:T(8,128)(2,1)} %all-gather.9.cloned.1.call-done, bf16[384,2048]{0,1:T(8,128)(2,1)S(1)} %fusion.2), kind=kOutput, calls=%fused_computation.37 | convolution fusion | flops 1209974784 | bytes 9437184 | tf_op jit(solution)/shard_map/dot_general | solution.py:106
  200.3 26.5 %all_to_all.23 = bf16[8,384,256]{2,1,0:T(8,128)(2,1)S(1)} all-to-all(bf16[8,384,256]{2,1,0:T(8,128)(2,1)S(1)} %bitcast.99), channel_id=1, replica_groups=mesh['rep'=2,'fs'=32,'tp_0'=4,'tp_1'=2] {'tp_0','tp_1'}, dimensions={0} | all-to-all | bytes 3145728 | tf_op jit(solution)/shard_map/all_to_all | solution.py:90
  (46 shorter events, 12.1 us)
Async XLA Ops:
  6.5 0.8 copy-start
  6.5 90.6 %all-gather.7.cloned.1.call-start = ((), (), s32[]{:S(2)}) async-start(), calls=%async_computation.4 | async-start | bytes 3194880 | tf_op jit(solution)/shard_map/all_gather | solution.py:56
  8.7 181.3 %all-gather.9.cloned.1.call-start = ((), (), s32[]{:S(2)}) async-start(), calls=%async_computation.5 | async-start | bytes 6389760 | tf_op jit(solution)/shard_map/all_gather | solution.py:56
  32.6 13.2 %copy-start.1 = (bf16[4,2,192,256]{3,2,1,0:T(8,128)(2,1)}, bf16[4,2,192,256]{3,2,1,0:T(8,128)(2,1)S(1)}, u32[]{:S(2)}) copy-start(bf16[4,2,192,256]{3,2,1,0:T(8,128)(2,1)S(1)} %copy.52) | copy-start | bytes 2359300
  45.8 0.9 copy-start.2
  48.9 7.2 %copy-start.4 = (f32[2048]{0:T(1024)S(1)}, f32[2048]{0:T(1024)}, u32[]{:S(2)}) copy-start(f32[2048]{0:T(1024)} %param.11) | copy-start | bytes 24580
  109.0 13.3 %all-to-all-start = ((f32[8,1,768]{2,1,0:T(1,128)}), f32[8,1,768]{2,1,0:T(1,128)S(1)}, u32[]{:S(2)}, u32[]{:S(2)}) async-start(f32[8,1,768]{2,1,0:T(1,128)} %broadcast_in_dim.4), calls=%async_computation | async-start | bytes 49152 | tf_op jit(solution)/shard_map/all_to_all | solution.py:67
  123.3 24.0 %copy-start.3 = (bf16[384,256]{1,0:T(8,128)(2,1)S(1)}, bf16[384,256]{1,0:T(8,128)(2,1)}, u32[]{:S(2)}) copy-start(bf16[384,256]{1,0:T(8,128)(2,1)} %param.10) | copy-start | bytes 589828
  147.7 24.5 %copy-start.5 = (f32[2048]{0:T(1024)S(1)}, f32[2048]{0:T(1024)}, u32[]{:S(2)}) copy-start(f32[2048]{0:T(1024)} %param.17) | copy-start | bytes 24580
Sparse Core Ops, SparseCore 0:
  10.3 86.7 all-gather.6
  100.2 89.7 all-gather.8
where the time goes:
time: 236 us; the launch traced here: 235 us
  blocking collectives  109 us (46%)
  waiting for transfers between devices  59.6 us (25%)
  matrix products  17.2 us (7%)
  local copies, waits for them, and re-layouts  14.1 us (6%)
  between operations  13.6 us (6%)
  other arithmetic  12.5 us (5%)
  starting transfers between devices  8.62 us (4%)
    all_gather x2, waiting for transfers between devices, whole_halves(): pieces = lax.all_gather(mine, ('rep', 'fs'), axis=0, tiled=True)  56.3 us
    all_to_all x2, blocking collectives, summed_on_arrival(): lax.all_to_all(in_blocks(shard, dim, count), axis, 0, 0, tiled=True)  50.3 us
    all_gather x4, blocking collectives, gather_in_order(): pieces = lax.all_gather(pieces, axes[k])  34.5 us
    all_to_all x1, blocking collectives, copy_for_each(): return lax.all_to_all(copies, axis, split_axis=0, concat_axis=0, tiled=True)  24.1 us
    dot_general x3, matrix products, times_transposed(): lax.dot_general(left, right, (((1,), (1,)), ((), ())), preferred_element_...  10.8 us
    all_to_all x1, starting transfers between devices, copy_for_each(): return lax.all_to_all(copies, axis, split_axis=0, concat_axis=0, tiled=True)  8.58 us
  transfers between devices with their start and end apart: 3, of which 3 were waited for; matrix products, arithmetic and copies ran while one was open for 13% of the time, Pallas kernels for 0%

commit v1 on v0

--- a/solution.py
+++ b/solution.py
@@ -9,6 +9,13 @@
 LENGTH = 128
 TP = ("tp_0", "tp_1")
 EPS = 1e-06
+
+
+def exchange_gather(x, axis, along):
+    devices = lax.axis_size(axis)
+    blocks = jnp.stack([x for _ in range(devices)])
+    blocks = lax.all_to_all(blocks, axis, split_axis=0, concat_axis=0)
+    return jnp.concatenate(blocks, axis=along)
 
 
 def cut_rows(length, count):
@@ -53,7 +60,7 @@
 
 def whole_halves(weights):
     mine = jnp.concatenate([half_of(w) for w in weights], axis=1)
-    pieces = lax.all_gather(mine, ("rep", "fs"), axis=0, tiled=True)
+    pieces = exchange_gather(mine, ("rep", "fs"), 0)
     pieces = pieces.reshape(2, -1, mine.shape[1])
     ends, at = ([], 0)
     for w in weights[:-1]:

time: 236 us -> 454 us (1.92)
  the two profiles are of different devices: /device:TPU:1 before, /device:TPU:40 now
where the time goes in v1:
time: 454 us; the launch traced here: 453 us
  waiting for transfers between devices  286 us (63%)
  blocking collectives  78.9 us (17%)
  starting transfers between devices  32.2 us (7%)
  local copies, waits for them, and re-layouts  28.7 us (6%)
  matrix products  14.2 us (3%)
  other arithmetic  12.4 us (3%)
    all_to_all x2, waiting for transfers between devices, exchange_gather(): blocks = lax.all_to_all(blocks, axis, split_axis=0, concat_axis=0)  261 us
    all_to_all x2, blocking collectives, summed_on_arrival(): lax.all_to_all(in_blocks(shard, dim, count), axis, 0, 0, tiled=True)  48 us
    all_gather x4, blocking collectives, gather_in_order(): pieces = lax.all_gather(pieces, axes[k])  30.8 us
    all_to_all x2, waiting for transfers between devices, copy_for_each(): return lax.all_to_all(copies, axis, split_axis=0, concat_axis=0, tiled=True)  24.8 us
    all_to_all x2, starting transfers between devices, exchange_gather(): blocks = lax.all_to_all(blocks, axis, split_axis=0, concat_axis=0)  24.2 us
    dot_general x3, matrix products, times_transposed(): lax.dot_general(left, right, (((1,), (1,)), ((), ())), preferred_element_...  11.9 us
  transfers between devices with their start and end apart: 4, of which 4 were waited for; matrix products, arithmetic and copies ran while one was open for 3% of the time, Pallas kernels for 0%

profile of v1, /device:TPU:40, one launch (start us, length us, event | category | flops | bytes accessed | tf_op | source)
XLA Modules:
  0.0 452.7 jit_solution(2299130367446912522)
XLA Ops:
  1.5 2.2 stack.4
  3.7 16.4 %all-to-all-start = ((bf16[64,64,384]{2,1,0:T(8,128)(2,1)}), bf16[64,64,384]{2,1,0:T(8,128)(2,1)}, u32[]{:S(2)}, u32[]{:S(2)}) async-start(bf16[64,64,384]{2,1,0:T(8,128)(2,1)} %stack.4), calls=%async_computation | async-start | bytes 6291456 | tf_op jit(solution)/shard_map/all_to_all | solution.py:17
  20.2 12.9 %all-gather = bf16[768,256]{1,0:T(8,128)(2,1)S(1)} all-gather(bf16[192,256]{1,0:T(8,128)(2,1)S(1)} %get-tuple-element.43), channel_id=2, replica_groups=mesh['rep'=2,'fs'=32,'tp_0'=4,'tp_1'=2] {'tp_0'}, dimensions={0}, use_global_device_ids=true | all-gather | bytes 491520 | tf_op jit(solution)/shard_map/all_gather | solution.py:31
  33.0 2.4 all-gather.1
  35.5 1.9 all-gather.2
  37.4 13.7 %all-gather.3 = bf16[8,192,256]{2,1,0:T(8,128)(2,1)S(1)} all-gather(bf16[2,192,256]{2,1,0:T(8,128)(2,1)S(1)} %bitcast.116), channel_id=5, replica_groups=mesh['rep'=2,'fs'=32,'tp_0'=4,'tp_1'=2] {'tp_0'}, dimensions={0}, use_global_device_ids=true | all-gather | bytes 983040 | tf_op jit(solution)/shard_map/all_gather | solution.py:31
  52.2 1.8 copy.52
  54.1 2.4 reshape.151
  60.7 2.2 multiply_convert_fusion
  62.9 52.8 %all-to-all-done = bf16[64,64,384]{2,1,0:T(8,128)(2,1)} async-done(((bf16[64,64,384]{2,1,0:T(8,128)(2,1)}), bf16[64,64,384]{2,1,0:T(8,128)(2,1)}, u32[]{:S(2)}, u32[]{:S(2)}) %all-to-all-start) | async-done | bytes 3145760 | tf_op jit(solution)/shard_map/all_to_all | solution.py:17
  115.7 2.2 fusion.112
  120.5 4.5 %fusion.109 = (f32[3,128]{1,0:T(4,128)S(1)}, f32[3,128]{1,0:T(4,128)S(1)}, f32[3,128,256]{1,2,0:T(8,128)S(1)}) fusion(f32[3,128,256]{1,2,0:T(8,128)S(1)} %maximum_multiply_fusion, f32[256]{0:T(256)S(1)} %bitcast.131, f32[256]{0:T(256)S(1)} %bitcast.133, f32[256]{0:T(256)S(1)} %bitcast.134, f32[256]{0:T(256)S(1)} %bitcast.135, f32[256]{0:T(256)S(1)} %bitcast.136, ...), kind=kLoop, calls=%fused_computation.159 | loop fusion | flops 6290688 | bytes 821248 | tf_op jit(solution)/shard_map/reduce_sum | solution.py:142
  125.7 4.3 all-to-all-start.1
  132.0 3.4 all-to-all-done.1
  136.3 24.0 %all_to_all.31 = bf16[8,384,256]{2,1,0:T(8,128)(2,1)S(1)} all-to-all(bf16[8,384,256]{2,1,0:T(8,128)(2,1)S(1)} %bitcast.102), channel_id=1, replica_groups=mesh['rep'=2,'fs'=32,'tp_0'=4,'tp_1'=2] {'tp_0','tp_1'}, dimensions={0} | all-to-all | bytes 3145728 | tf_op jit(solution)/shard_map/all_to_all | solution.py:97
  162.8 3.7 all-to-all-start.3
  166.6 21.4 %all-to-all-done.3 = bf16[8,384,256]{1,2,0:T(8,128)(2,1)S(1)} async-done(((bf16[8,384,256]{1,2,0:T(8,128)(2,1)}), bf16[8,384,256]{1,2,0:T(8,128)(2,1)S(1)}, u32[]{:S(2)}, u32[]{:S(2)}) %all-to-all-start.3) | async-done | bytes 1572896 | tf_op jit(solution)/shard_map/all_to_all | solution.py:74
  188.0 3.4 stack.5
  191.4 7.8 %all-to-all-start.4 = ((bf16[64,64,768]{2,1,0:T(8,128)(2,1)}), bf16[64,64,768]{2,1,0:T(8,128)(2,1)}, u32[]{:S(2)}, u32[]{:S(2)}) async-start(bf16[64,64,768]{2,1,0:T(8,128)(2,1)} %stack.5), calls=%async_computation.4 | async-start | bytes 12582912 | tf_op jit(solution)/shard_map/all_to_all | solution.py:17
  201.5 208.3 %all-to-all-done.4 = bf16[64,64,768]{2,1,0:T(8,128)(2,1)} async-done(((bf16[64,64,768]{2,1,0:T(8,128)(2,1)}), bf16[64,64,768]{2,1,0:T(8,128)(2,1)}, u32[]{:S(2)}, u32[]{:S(2)}) %all-to-all-start.4) | async-done | bytes 6291488 | tf_op jit(solution)/shard_map/all_to_all | solution.py:17
  409.8 5.1 %fusion.111 = (bf16[32,64,768]{2,1,0:T(8,128)(2,1)S(1)}, bf16[32,64,768]{2,1,0:T(8,128)(2,1)}) fusion(bf16[64,64,768]{2,1,0:T(8,128)(2,1)} %all-to-all-done.4), kind=kLoop, calls=%fused_computation.160 | loop fusion | bytes 12582912 | tf_op jit(solution)/shard_map/slice | solution.py:69
  414.9 5.9 %fusion.6 = f32[384,2048]{1,0:T(8,128)} fusion(bf16[2048,768]{1,0:T(8,128)(2,1)} %bitcast.113, bf16[384,2048]{0,1:T(8,128)(2,1)} %fusion.2), kind=kOutput, calls=%fused_computation.47 | convolution fusion | flops 1208401920 | bytes 7864320 | tf_op jit(solution)/shard_map/dot_general | solution.py:113
  420.8 5.4 %add_convert_fusion = bf16[384,2048]{1,0:T(8,128)(2,1)} fusion(f32[384,2048]{1,0:T(8,128)} %fusion.6, bf16[2048,768]{1,0:T(8,128)(2,1)S(1)} %bitcast.112, bf16[384,2048]{0,1:T(8,128)(2,1)} %fusion.2), kind=kOutput, calls=%fused_computation.37 | convolution fusion | flops 1209974784 | bytes 9437184 | tf_op jit(solution)/shard_map/dot_general | solution.py:113
  427.7 24.0 %all_to_all.32 = bf16[8,384,256]{2,1,0:T(8,128)(2,1)S(1)} all-to-all(bf16[8,384,256]{2,1,0:T(8,128)(2,1)S(1)} %bitcast.103), channel_id=1, replica_groups=mesh['rep'=2,'fs'=32,'tp_0'=4,'tp_1'=2] {'tp_0','tp_1'}, dimensions={0} | all-to-all | bytes 3145728 | tf_op jit(solution)/shard_map/all_to_all | solution.py:97
  (58 shorter events, 20.2 us)
Async XLA Ops:
  0.0 0.8 copy-start
  3.7 16.4 %copy-start.4 = (bf16[384,256]{1,0:T(8,128)(2,1)S(1)}, bf16[384,256]{1,0:T(8,128)(2,1)}, u32[]{:S(2)}) copy-start(bf16[384,256]{1,0:T(8,128)(2,1)} %param.10) | copy-start | bytes 589828
  3.7 112.0 %all-to-all-start = ((bf16[64,64,384]{2,1,0:T(8,128)(2,1)}), bf16[64,64,384]{2,1,0:T(8,128)(2,1)}, u32[]{:S(2)}, u32[]{:S(2)}) async-start(bf16[64,64,384]{2,1,0:T(8,128)(2,1)} %stack.4), calls=%async_computation | async-start | bytes 6291456 | tf_op jit(solution)/shard_map/all_to_all | solution.py:17
  35.5 15.6 %copy-start.1 = (bf16[4,2,192,256]{3,2,1,0:T(8,128)(2,1)}, bf16[4,2,192,256]{3,2,1,0:T(8,128)(2,1)S(1)}, u32[]{:S(2)}) copy-start(bf16[4,2,192,256]{3,2,1,0:T(8,128)(2,1)S(1)} %copy.51) | copy-start | bytes 2359300
  51.1 0.9 copy-start.2
  56.5 4.2 copy-start.8
  117.9 1.2 copy-start.3
  125.7 9.7 %all-to-all-start.1 = ((f32[8,1,768]{2,1,0:T(1,128)}), f32[8,1,768]{2,1,0:T(1,128)S(1)}, u32[]{:S(2)}, u32[]{:S(2)}) async-start(f32[8,1,768]{2,1,0:T(1,128)} %broadcast_in_dim.4), calls=%async_computation.1 | async-start | bytes 49152 | tf_op jit(solution)/shard_map/all_to_all | solution.py:74
  160.4 0.9 copy-start.5
  162.8 3.7 copy-start.6
  162.8 3.7 copy-start.7
  162.8 25.2 %all-to-all-start.3 = ((bf16[8,384,256]{1,2,0:T(8,128)(2,1)}), bf16[8,384,256]{1,2,0:T(8,128)(2,1)S(1)}, u32[]{:S(2)}, u32[]{:S(2)}) async-start(bf16[8,384,256]{1,2,0:T(8,128)(2,1)} %broadcast_in_dim.5), calls=%async_computation.3 | async-start | bytes 3145728 | tf_op jit(solution)/shard_map/all_to_all | solution.py:74
  191.4 218.4 %all-to-all-start.4 = ((bf16[64,64,768]{2,1,0:T(8,128)(2,1)}), bf16[64,64,768]{2,1,0:T(8,128)(2,1)}, u32[]{:S(2)}, u32[]{:S(2)}) async-start(bf16[64,64,768]{2,1,0:T(8,128)(2,1)} %stack.5), calls=%async_computation.4 | async-start | bytes 12582912 | tf_op jit(solution)/shard_map/all_to_all | solution.py:17
  199.2 0.7 copy-start.9
